TPU v7x, 32 devices: a whole 2x2x4 slice. The times are simulated.
32 devices in a mesh: sp: 8 (over z, x), tp: 4 (over y, core).
Axes of the slice: x: 2, y: 2, z: 4, core: 2. Of those that a mesh axis runs over, the one named last changes fastest.
Arguments:
- tokens: bfloat16 [3072, 2048], P(('sp', 'tp')), may hold values from -6 to 6
- norm_gain: bfloat16 [2048], replicated, may hold values from 0.099609375 to 1.8984375
- query_down_weight: bfloat16 [2048, 512], replicated, may hold values from -0.125 to 0.125
- query_latent_norm_gain: bfloat16 [512], replicated, may hold values from 0.099609375 to 1.8984375
- key_value_down_weight: bfloat16 [2048, 256], replicated, may hold values from -0.125 to 0.125
- key_value_latent_gain: bfloat16 [256], replicated, may hold values from 0.099609375 to 1.8984375
- w_rope_key: bfloat16 [2048, 32], replicated, may hold values from -0.125 to 0.125
- w_pool_in: bfloat16 [2048, 512], replicated, may hold values from -0.125 to 0.125
- query_up_weight: bfloat16 [512, 2304], P(None, 'tp'), may hold values from -0.25 to 0.25
- key_value_up_weight: bfloat16 [256, 3072], P(None, 'tp'), may hold values from -0.375 to 0.375
- query_gain: bfloat16 [96], replicated, may hold values from 1 to 16
- key_gain: bfloat16 [96], replicated, may hold values from 1 to 16
- w_pool_mix: bfloat16 [8, 64, 64], P('tp'), may hold values from -0.75 to 0.75
- pool_scale: bfloat16 [512], P('tp'), may hold values from 1 to 10
- w_out_attn: bfloat16 [1536, 2048], P('tp'), may hold values from -0.3125 to 0.3125
- w_out_pool: bfloat16 [512, 2048], P('tp'), may hold values from -0.25 to 0.25
Outputs:
- mixed: bfloat16 [3072, 2048], P(('sp', 'tp'))
- row_logsum: float32 [24, 3072], P('tp', 'sp')
All inputs are finite; a program needn't handle non-finite values.
Results may differ from a plain program's by a relative error of at most 0.035.
Values may be sent and summed in bfloat16 or wider, within the bound.
A program may use at most 128 MiB of HBM per device.

v0:
```python
import jax
import jax.numpy as jnp
from jax import lax
from jax.sharding import PartitionSpec as P

PLAIN_HEAD_SIZE = 64
ROTARY_SIZE = 32
VALUE_HEAD_SIZE = 64
QUERY_RANK = 512
KEY_VALUE_RANK = 256
GDIM = 64


epsilon = 1e-06
rope_base = 10000.0
rim_width = 8


def with_halo(block, sides, width):
    for axis, dim in sides:
        count = lax.axis_size(axis)
        forward = [(i, i + 1) for i in range(count - 1)]
        backward = [(target, source) for source, target in forward]
        low = lax.ppermute(
            lax.slice_in_dim(block, block.shape[dim] - width, None, axis=dim), axis, forward
        )
        high = lax.ppermute(lax.slice_in_dim(block, 0, width, axis=dim), axis, backward)
        block = jnp.concatenate([low, block, high], axis=dim)
    return block


def norm_rows(values, gain):
    mean_square = jnp.mean(values * values, axis=-1, keepdims=True)
    return values * lax.rsqrt(mean_square + epsilon) * gain.astype(jnp.float32)


def rotate_tail(values, positions):
    half = ROTARY_SIZE // 2
    freqs = rope_base ** (-jnp.arange(half, dtype=jnp.float32) / half)
    angles = positions[:, None] * freqs[None, :]
    cosine = jnp.cos(angles)[:, None, :]
    sine = jnp.sin(angles)[:, None, :]
    first = values[..., PLAIN_HEAD_SIZE : PLAIN_HEAD_SIZE + half]
    second = values[..., PLAIN_HEAD_SIZE + half :]
    return jnp.concatenate(
        [
            values[..., :PLAIN_HEAD_SIZE],
            first * cosine - second * sine,
            first * sine + second * cosine,
        ],
        axis=-1,
    )


def shards(
    tokens,
    norm_gain,
    query_down_weight,
    query_latent_norm_gain,
    key_value_down_weight,
    key_value_latent_gain,
    w_rope_key,
    w_pool_in,
    query_up_weight,
    key_value_up_weight,
    query_gain,
    key_gain,
    w_pool_mix,
    pool_scale,
    w_out_attn,
    w_out_pool,
):
    sp_count = lax.axis_size("sp")
    local_heads = query_up_weight.shape[1] // (PLAIN_HEAD_SIZE + ROTARY_SIZE)
    groups_here = w_pool_mix.shape[0]
    pool_cols = groups_here * GDIM
    latent_columns = QUERY_RANK + KEY_VALUE_RANK + ROTARY_SIZE
    pool_weight = lax.dynamic_slice_in_dim(
        w_pool_in, lax.axis_index("tp") * pool_cols, pool_cols, 1
    )
    normed = norm_rows(
        lax.all_gather(tokens, "tp", axis=0, tiled=True).astype(jnp.float32), norm_gain
    ).astype(jnp.bfloat16)
    pool_part = jnp.dot(normed, pool_weight, preferred_element_type=jnp.float32).astype(
        jnp.bfloat16
    )
    query_part = norm_rows(
        jnp.dot(normed, query_down_weight, preferred_element_type=jnp.float32),
        query_latent_norm_gain,
    )
    kv_part = norm_rows(
        jnp.dot(normed, key_value_down_weight, preferred_element_type=jnp.float32),
        key_value_latent_gain,
    )
    rope_part = jnp.dot(normed, w_rope_key, preferred_element_type=jnp.float32)
    projected = jnp.concatenate(
        [
            jnp.concatenate(
                [
                    query_part.astype(jnp.bfloat16),
                    kv_part.astype(jnp.bfloat16),
                    rope_part.astype(jnp.bfloat16),
                ],
                axis=1,
            ),
            pool_part,
        ],
        axis=1,
    )
    latent_vectors = projected[:, :latent_columns]
    pool_input = projected[:, latent_columns:]
    rows = latent_vectors.shape[0]
    offset = lax.axis_index("sp") * rows
    places = offset + jnp.arange(rows, dtype=jnp.int32)
    positions = places.astype(jnp.float32)
    query_vectors = jnp.dot(
        latent_vectors[:, :QUERY_RANK], query_up_weight, preferred_element_type=jnp.float32
    ).reshape(rows, local_heads, PLAIN_HEAD_SIZE + ROTARY_SIZE)
    query_vectors = rotate_tail(norm_rows(query_vectors, query_gain), positions).astype(
        jnp.bfloat16
    )
    key_value_rows = latent_vectors[:, QUERY_RANK:]
    scale = (PLAIN_HEAD_SIZE + ROTARY_SIZE) ** (-0.5)

    def keys_of(latent_rows, key_positions):
        total_count = latent_rows.shape[0]
        key_value_pair = jnp.dot(
            latent_rows[:, :KEY_VALUE_RANK], key_value_up_weight, preferred_element_type=jnp.float32
        ).reshape(total_count, local_heads, PLAIN_HEAD_SIZE + VALUE_HEAD_SIZE)
        shared = jnp.broadcast_to(
            latent_rows[:, None, KEY_VALUE_RANK:].astype(jnp.float32),
            (total_count, local_heads, ROTARY_SIZE),
        )
        keys = jnp.concatenate([key_value_pair[..., :PLAIN_HEAD_SIZE], shared], axis=-1)
        keys = rotate_tail(norm_rows(keys, key_gain), key_positions).astype(jnp.bfloat16)
        return (keys, key_value_pair[..., PLAIN_HEAD_SIZE:].astype(jnp.bfloat16))

    def absorb(carry, keys, values):
        row_max, row_total, accum = carry
        scores = (
            jnp.einsum("qhd,khd->hqk", query_vectors, keys, preferred_element_type=jnp.float32)
            * scale
        )
        new_max = jnp.maximum(row_max, jnp.max(scores, axis=-1))
        factor = jnp.exp(row_max - new_max)
        exp_scores = jnp.exp(scores - new_max[:, :, None])
        row_total = row_total * factor + jnp.sum(exp_scores, axis=-1)
        summed = jnp.einsum(
            "hqk,khd->qhd",
            exp_scores.astype(jnp.bfloat16),
            values,
            preferred_element_type=jnp.float32,
        )
        accum = accum * jnp.transpose(factor)[:, :, None] + summed
        return (new_max, row_total, accum)

    initial = (
        jnp.full((local_heads, rows), -1e30, jnp.float32),
        jnp.zeros((local_heads, rows), jnp.float32),
        jnp.zeros((rows, local_heads, VALUE_HEAD_SIZE), jnp.float32),
    )

    def take_latents(carry, block, block_start):
        key_positions = (block_start + jnp.arange(rows, dtype=jnp.int32)).astype(jnp.float32)
        keys, values = keys_of(block, key_positions)
        return absorb(carry, keys, values)

    carry = initial
    piece = lax.all_gather(key_value_rows, "sp", axis=0, tiled=True)
    run_total_count = piece.shape[0] // rows
    stacked = piece.reshape((run_total_count, rows) + piece.shape[1:])

    def one_block(carry_in, pair):
        block, number = pair
        return (take_latents(carry_in, block, number * rows), None)

    carry, unused = lax.scan(
        one_block, carry, (stacked, jnp.arange(run_total_count, dtype=jnp.int32))
    )
    row_max, row_total, accum = carry
    attention = (
        (accum / jnp.transpose(row_total)[:, :, None])
        .astype(jnp.bfloat16)
        .reshape(rows, local_heads * VALUE_HEAD_SIZE)
    )
    row_logsum = row_max + jnp.log(row_total)
    padded = with_halo(pool_input, (("sp", 0),), rim_width)
    running = jnp.concatenate(
        [jnp.zeros((1, pool_cols), jnp.float32), jnp.cumsum(padded.astype(jnp.float32), axis=0)],
        axis=0,
    )
    length = rows * sp_count
    pieces = []
    for local in range(groups_here):
        group = lax.axis_index("tp") * groups_here + local
        half = jnp.left_shift(jnp.int32(1), group % 4)
        first_col = local * GDIM
        upper_sum = lax.dynamic_slice_in_dim(running, rim_width + half, rows, 0)[
            :, first_col : first_col + GDIM
        ]
        lower_sum = lax.dynamic_slice_in_dim(running, rim_width - half, rows, 0)[
            :, first_col : first_col + GDIM
        ]
        total_count = (jnp.minimum(places + half, length) - jnp.maximum(places - half, 0)).astype(
            jnp.float32
        )[:, None]
        pooled = (
            (upper_sum - lower_sum) / total_count
            - pool_input[:, first_col : first_col + GDIM].astype(jnp.float32)
        ).astype(jnp.bfloat16)
        mapped = jnp.dot(pooled, w_pool_mix[local], preferred_element_type=jnp.float32)
        pieces.append(
            (mapped * pool_scale[first_col : first_col + GDIM].astype(jnp.float32)).astype(
                jnp.bfloat16
            )
        )
    pool_out = jnp.concatenate(pieces, axis=1)
    mixed = lax.psum_scatter(
        (
            jnp.dot(attention, w_out_attn, preferred_element_type=jnp.float32)
            + jnp.dot(pool_out, w_out_pool, preferred_element_type=jnp.float32)
        ).astype(jnp.bfloat16),
        "tp",
        scatter_dimension=0,
        tiled=True,
    )
    return (mixed, row_logsum)


def solution(mesh):
    placed = (
        P(("sp", "tp"), None),
        P(),
        P(),
        P(),
        P(),
        P(),
        P(),
        P(),
        P(None, "tp"),
        P(None, "tp"),
        P(),
        P(),
        P("tp", None, None),
        P("tp"),
        P("tp", None),
        P("tp", None),
    )
    return jax.shard_map(
        shards,
        mesh=mesh,
        in_specs=placed,
        out_specs=(P(("sp", "tp"), None), P("tp", "sp")),
        check_vma=False,
    )
```

profile of v0, /device:TPU:0, one launch (start us, length us, event | category | flops | bytes accessed | tf_op | source)
XLA Modules:
  0.0 176.3 jit_solution(6229357803889036211)
XLA Ops:
  7.2 0.7 all-gather.3.cloned.1.call-update
  8.0 0.7 convert_element_type.114
  8.7 0.7 convert_element_type.109
  9.4 0.7 convert_element_type.112
  10.0 0.7 convert_element_type.107
  11.4 1.3 slice_convert_fusion.6
  12.7 0.8 multiply_cosine_fusion.1
  13.5 18.5 %all-gather.3.cloned.1.call-done = bf16[384,2048]{1,0:T(8,128)(2,1)} async-done(((bf16[96,2048]{1,0:T(8,128)(2,1)}), bf16[384,2048]{1,0:T(8,128)(2,1)}) %all-gather.3.cloned.1.call-update) | async-done | bytes 1572880 | tf_op jit(solution)/shard_map/all_gather | solution.py:82
  31.9 1.9 %fusion.25 = f32[384]{0:T(512)S(1)} fusion(bf16[384,2048]{1,0:T(8,128)(2,1)} %all-gather.3.cloned.1.call-done), kind=kLoop, calls=%fused_computation.42 | loop fusion | flops 2358912 | bytes 1574400 | tf_op jit(solution)/shard_map/reduce_sum | solution.py:33
  33.9 2.1 %convolution_convert_fusion = bf16[384,128]{1,0:T(8,128)(2,1)S(1)} fusion(bf16[2048,512]{1,0:T(8,128)(2,1)} %param.25, s32[]{:T(128)S(6)} %select_n.26, bf16[384,2048]{1,0:T(8,128)(2,1)} %all-gather.3.cloned.1.call-done, f32[2048]{0:T(1024)S(1)} %convert_element_type.107, f32[384]{0:T(512)S(1)} %add_rsqrt_fusion.4), kind=kOutput, calls=%fused_computation.49 | convolution fusion | flops 204521472 | bytes 2205188 | tf_op jit(solution)/shard_map/dot_general | solution.py:84
  36.7 3.4 %collective-permute-start = (bf16[8,128]{1,0:T(8,128)(2,1)}, bf16[8,128]{1,0:T(8,128)(2,1)S(1)}, u32[]{:S(2)}, u32[]{:S(2)}) collective-permute-start(bf16[8,128]{1,0:T(8,128)(2,1)} %get-tuple-element.130), channel_id=1, source_target_pairs={{0,4},{4,8},{8,12},{12,16},{16,20},{20,24},{24,28},{1,5},{5,9},{9,... | collective-permute-start | bytes 6152 | tf_op jit(solution)/shard_map/ppermute | solution.py:24
  40.0 1.3 collective-permute-start.1
  41.4 0.9 multiply_reduce_fusion.3
  42.4 0.6 convolution_convert_fusion.1
  43.0 0.7 pad_maximum_fusion.2
  43.9 2.6 %multiply_reduce_fusion.2 = (f32[384]{0:T(512)S(1)}, f32[384,512]{1,0:T(8,128)S(1)}) fusion(bf16[2048,512]{1,0:T(8,128)(2,1)S(1)} %copy-done, bf16[384,2048]{1,0:T(8,128)(2,1)} %all-gather.3.cloned.1.call-done, f32[2048]{0:T(1024)S(1)} %convert_element_type.107, f32[384]{0:T(512)S(1)} %add_rsqrt_fusion.4), kind=kOutput, calls=%fused_computation.56 | convolution fusion | flops 808844928 | bytes 4467712 | tf_op jit(solution)/shard_map/dot_general | solution.py:88
  47.9 1.2 fusion.28
  49.1 1.3 fusion.29
  50.4 2.3 %fusion.42 = f32[384,2048]{1,0:T(8,128)} fusion(bf16[128,2048]{1,0:T(8,128)(2,1)S(1)} %copy-done.4, bf16[384,64]{1,0:T(8,128)(2,1)S(1)} %fusion.29, bf16[384,64]{1,0:T(8,128)(2,1)S(1)} %fusion.28), kind=kOutput, calls=%fused_computation.81 | convolution fusion | flops 201523200 | bytes 3768320 | tf_op jit(solution)/shard_map/dot_general | solution.py:221
  52.7 39.1 %all-gather.5.cloned.1.call-done = bf16[3072,288]{0,1:T(8,128)(2,1)} async-done(((bf16[384,288]{0,1:T(8,128)(2,1)}), bf16[3072,288]{0,1:T(8,128)(2,1)}) %all-gather.5.cloned.1.call-update) | async-done | bytes 1769488 | tf_op jit(solution)/shard_map/all_gather | solution.py:169
  91.8 2.9 %copy.35 = bf16[36,8,8,384]{3,2,0,1:T(8,128)(2,1)} copy(bf16[36,8,8,384]{3,2,1,0:T(8,128)(2,1)} %bitcast.83) | data formatting | bytes 3538944 | tf_op jit(solution)/shard_map/reshape | solution.py:171
  94.7 44.1 %while.15 = (s32[]{:T(128)}, f32[6,384]{1,0:T(8,128)S(1)}, f32[6,384]{1,0:T(8,128)S(1)}, f32[384,6,64]{0,2,1:T(8,128)S(1)}, bf16[8,384,288]{1,2,0:T(8,128)(2,1)}...) while((s32[]{:T(128)}, f32[6,384]{1,0:T(8,128)S(1)}, ...), condition=%wide.region_8.9_spmd.clone, body=%wide.region_4.8_spmd.clone.sunk | while | flops 444615296 | bytes 20764904 | solution.py:177
  96.1 1.0 dynamic-slice_bitcast_fusion.2
  98.0 0.7 bitcast_reduce_fusion.2
  98.7 0.8 fusion.91
  101.7 1.0 dynamic-slice_bitcast_fusion.2
  103.5 0.7 bitcast_reduce_fusion.2
  104.2 0.8 fusion.91
  107.2 1.0 dynamic-slice_bitcast_fusion.2
  109.0 0.7 bitcast_reduce_fusion.2
  109.7 0.8 fusion.91
  112.7 1.0 dynamic-slice_bitcast_fusion.2
  114.5 0.7 bitcast_reduce_fusion.2
  115.3 0.8 fusion.91
  118.2 1.0 dynamic-slice_bitcast_fusion.2
  120.1 0.7 bitcast_reduce_fusion.2
  120.8 0.8 fusion.91
  123.7 1.0 dynamic-slice_bitcast_fusion.2
  125.6 0.7 bitcast_reduce_fusion.2
  126.3 0.8 fusion.91
  129.2 1.0 dynamic-slice_bitcast_fusion.2
  131.1 0.7 bitcast_reduce_fusion.2
  131.8 0.8 fusion.91
  134.8 1.0 dynamic-slice_bitcast_fusion.2
  136.6 0.7 bitcast_reduce_fusion.2
  137.3 0.8 fusion.91
  138.9 4.5 %add_convert_fusion.2 = bf16[384,2048]{1,0:T(8,128)(2,1)} fusion(f32[384,2048]{1,0:T(8,128)} %fusion.42, bf16[384,384]{0,1:T(8,128)(2,1)S(1)} %bitcast.84, bf16[384,2048]{1,0:T(8,128)(2,1)} %param.32), kind=kOutput, calls=%fused_computation.45 | convolution fusion | flops 605552640 | bytes 6586368 | tf_op jit(solution)/shard_map/dot_general | solution.py:220
  144.0 25.8 %reduce-scatter.2.cloned.1.call-done = bf16[96,2048]{1,0:T(8,128)(2,1)} async-done(((bf16[384,2048]{1,0:T(8,128)(2,1)}), bf16[96,2048]{1,0:T(8,128)(2,1)}) %reduce-scatter.2.cloned.1.call-update) | async-done | bytes 393232 | tf_op jit(solution)/shard_map/reduce_scatter | solution.py:218
  (205 shorter events, 21.2 us)
Async XLA Ops:
  7.2 36.7 %copy-start = (bf16[2048,512]{1,0:T(8,128)(2,1)S(1)}, bf16[2048,512]{1,0:T(8,128)(2,1)}, u32[]{:S(2)}) copy-start(bf16[2048,512]{1,0:T(8,128)(2,1)} %param.20) | copy-start | bytes 6291460
  7.2 24.8 %all-gather.3.cloned.1.call-start = ((), (), s32[]{:S(2)}) async-start(), calls=%async_computation.1 | async-start | bytes 1966080 | tf_op jit(solution)/shard_map/all_gather | solution.py:82
  7.9 83.9 %all-gather.5.cloned.1.call-start = ((), (), s32[]{:S(2)}) async-start(), calls=%async_computation.2 | async-start | bytes 1990656 | tf_op jit(solution)/shard_map/all_gather | solution.py:169
  31.9 9.4 %copy-start.2 = (bf16[384,2048]{1,0:T(8,128)(2,1)S(1)}, bf16[384,2048]{1,0:T(8,128)(2,1)}, u32[]{:S(2)}) copy-start(bf16[384,2048]{1,0:T(8,128)(2,1)} %all-gather.3.cloned.1.call-done) | copy-start | bytes 4718596
  31.9 9.4 %copy-start.8 = (bf16[2048,256]{1,0:T(8,128)(2,1)S(1)}, bf16[2048,256]{1,0:T(8,128)(2,1)}, u32[]{:S(2)}) copy-start(bf16[2048,256]{1,0:T(8,128)(2,1)} %param.22) | copy-start | bytes 3145732
  36.0 4.0 %copy-start.5 = (bf16[384,128]{1,0:T(8,128)(2,1)}, bf16[384,128]{1,0:T(8,128)(2,1)S(1)}, u32[]{:S(2)}) copy-start(bf16[384,128]{1,0:T(8,128)(2,1)S(1)} %convolution_convert_fusion) | copy-start | bytes 294916
  36.1 6.3 %copy-start.9 = (bf16[2048,32]{0,1:T(8,128)(2,1)S(1)}, bf16[2048,32]{0,1:T(8,128)(2,1)}, u32[]{:S(2)}) copy-start(bf16[2048,32]{0,1:T(8,128)(2,1)} %param.24) | copy-start | bytes 393220
  36.7 10.8 %collective-permute-start = (bf16[8,128]{1,0:T(8,128)(2,1)}, bf16[8,128]{1,0:T(8,128)(2,1)S(1)}, u32[]{:S(2)}, u32[]{:S(2)}) collective-permute-start(bf16[8,128]{1,0:T(8,128)(2,1)} %get-tuple-element.130), channel_id=1, source_target_pairs={{0,4},{4,8},{8,12},{12,16},{16,20},{20,24},{24,28},{1,5},{5,9},{9,... | collective-permute-start | bytes 6152 | tf_op jit(solution)/shard_map/ppermute | solution.py:24
  40.0 7.4 %collective-permute-start.1 = (bf16[8,128]{1,0:T(8,128)(2,1)}, bf16[8,128]{1,0:T(8,128)(2,1)S(1)}, u32[]{:S(2)}, u32[]{:S(2)}) collective-permute-start(bf16[8,128]{1,0:T(8,128)(2,1)} %get-tuple-element.131), channel_id=1, source_target_pairs={{4,0},{8,4},{12,8},{16,12},{20,16},{24,20},{28,24},{5,1},{9,5},{13... | collective-permute-start | bytes 6152 | tf_op jit(solution)/shard_map/ppermute | solution.py:27
  43.8 2.7 %copy-start.3 = (bf16[512,576]{0,1:T(8,128)(2,1)S(1)}, bf16[512,576]{0,1:T(8,128)(2,1)}, u32[]{:S(2)}) copy-start(bf16[512,576]{0,1:T(8,128)(2,1)} %param.26) | copy-start | bytes 1769476
  43.8 126.0 %reduce-scatter.2.cloned.1.call-start = ((), (), s32[]{:S(2)}) async-start(), calls=%async_computation.3 | async-start | bytes 1966080 | tf_op jit(solution)/shard_map/reduce_scatter | solution.py:218
  46.4 0.9 copy-start.7
  46.5 1.0 copy-start.6
  47.8 2.6 %copy-start.4 = (bf16[128,2048]{1,0:T(8,128)(2,1)S(1)}, bf16[128,2048]{1,0:T(8,128)(2,1)}, u32[]{:S(2)}) copy-start(bf16[128,2048]{1,0:T(8,128)(2,1)} %param.33) | copy-start | bytes 1572868
  50.4 44.3 %copy-start.1 = (bf16[256,768]{1,0:T(8,128)(2,1)S(1)}, bf16[256,768]{1,0:T(8,128)(2,1)}, u32[]{:S(2)}) copy-start(bf16[256,768]{1,0:T(8,128)(2,1)} %param.27) | copy-start | bytes 1179652
  50.4 44.3 %copy-start.10 = (bf16[96]{0:T(256)(128)(2,1)S(1)}, bf16[96]{0:T(256)(128)(2,1)}, u32[]{:S(2)}) copy-start(bf16[96]{0:T(256)(128)(2,1)} %param.29) | copy-start | bytes 580
Sparse Core Ops, SparseCore 0:
  9.5 22.3 all-gather.2
  43.9 47.8 all-gather.4
  143.5 26.2 reduce-scatter.1
where the time goes:
time: 177 us; the launch traced here: 176 us
  waiting for transfers between devices  84.1 us (48%)
  matrix products  31.7 us (18%)
  other arithmetic  18.4 us (10%)
  local copies, waits for them, and re-layouts  16.9 us (10%)
  between operations  14.2 us (8%)
  loops' own time  6.39 us (4%)
  starting transfers between devices  4.77 us (3%)
    all_gather x1, waiting for transfers between devices, shards(): piece = lax.all_gather(key_value_rows, 'sp', axis=0, tiled=True)  39.1 us
    reduce_scatter x1, waiting for transfers between devices, shards(): lax.psum_scatter((jnp.dot(attention, w_out_attn, preferred_element_type=j...  25.8 us
    all_gather x1, waiting for transfers between devices, shards(): lax.all_gather(tokens, 'tp', axis=0, tiled=True).astype(jnp.float32)  18.5 us
    squeeze x8, local copies, waits for them, and re-layouts, shards(): lax.scan(one_block, carry, (stacked, jnp.arange(run_total_count, dtype=jn...  7.72 us
    dot_general x8, matrix products, absorb(): jnp.einsum('hqk,khd->qhd', exp_scores.astype(jnp.bfloat16), values, prefe...  6.76 us
    another operation x1, loops' own time, shards(): lax.scan(one_block, carry, (stacked, jnp.arange(run_total_count, dtype=jn...  6.39 us
    dot_general x8, matrix products, absorb(): jnp.einsum('qhd,khd->hqk', query_vectors, keys, preferred_element_type=jn...  5.5 us
    reduce_sum x8, other arithmetic, absorb(): row_total = row_total * factor + jnp.sum(exp_scores, axis=-1)  4.76 us
  transfers between devices with their start and end apart: 5, of which 3 were waited for; matrix products, arithmetic and copies ran while one was open for 10% of the time, Pallas kernels for 0%

commit v1 on v0

v1 whole, which is shorter than its diff:
```python
import functools

import jax
import jax.numpy as jnp
import numpy as np
from jax import lax
from jax.experimental import pallas as pl
from jax.experimental.pallas import tpu as pltpu
from jax.sharding import PartitionSpec as P

PLAIN = 64
ROT = 32
HEAD = PLAIN + ROT
VALUE = 64
GDIM = 64
EPS = 1e-06
ROPE_BASE = 10000.0
HALO = 16
F32 = jnp.float32
BF16 = jnp.bfloat16
MESH = pl.DeviceIdType.MESH
VMEM = pl.BlockSpec(memory_space=pltpu.VMEM)


def rms(x, width):
    return lax.rsqrt(jnp.sum(x * x, axis=-1, keepdims=True) * (1.0 / width) + EPS)


def mm(a, b):
    return jnp.dot(a, b, preferred_element_type=F32)


def gather_kernel(n_sp, n_tp, x_ref, gain_ref, wq_ref, qg_ref, wkv_ref, kvg_ref, wr_ref, wp_ref,
                  q_ref, pool_ref, kv_ref, pool_src,
                  kv_send, kv_recv, part_send, q_send, q_recv, p_send, p_recv, h_send, h_recv):
    sp = lax.axis_index("sp")
    tp = lax.axis_index("tp")
    n_dev = n_sp * n_tp
    n_ty = n_tp // 2
    n_chip = n_sp * n_ty
    me = sp * n_tp + tp
    core = lax.rem(tp, 2)
    ty = tp // 2
    partner = ty * 2 + 1 - core
    rows = x_ref.shape[0]
    pool_cols = pool_ref.shape[1]
    barrier = pltpu.get_barrier_semaphore()

    @pl.loop(1, n_dev)
    def _(i):
        d = lax.rem(me + i, n_dev)
        pl.semaphore_signal(barrier, inc=1, device_id=(d // n_tp, lax.rem(d, n_tp)), device_id_type=MESH)

    x = x_ref[...].astype(F32)
    normed = (x * rms(x, x.shape[1]) * gain_ref[...].astype(F32)).astype(BF16)
    kv = mm(normed, wkv_ref[...])
    kv_ref[me, :rows, :] = (kv * rms(kv, kv.shape[1]) * kvg_ref[...].astype(F32)).astype(BF16)
    rope = mm(normed, wr_ref[...])
    groups = rows // 16
    packed = [rope[16 * j : 16 * j + 16, :] for j in range(groups)]
    packed.append(jnp.zeros((16, kv.shape[1] - groups * ROT), F32))
    kv_ref[me, rows:, :] = jnp.concatenate(packed, axis=1).astype(BF16)
    pl.semaphore_wait(barrier, n_dev - 1)

    def chip_of(i):
        s = lax.rem(sp + i // n_ty, n_sp)
        t = lax.rem(ty + lax.rem(i, n_ty), n_ty) * 2 + core
        return s, t

    def source_of(i):
        s = lax.rem(sp + n_sp - i // n_ty, n_sp)
        t = lax.rem(ty + n_ty - lax.rem(i, n_ty), n_ty) * 2 + core
        return s * n_tp + t

    def kv_copy(slot, send_sem, target):
        return pltpu.make_async_remote_copy(
            src_ref=kv_ref.at[slot], dst_ref=kv_ref.at[slot], send_sem=send_sem,
            recv_sem=kv_recv.at[slot], device_id=target, device_id_type=MESH)

    @pl.loop(1, n_chip)
    def _(i):
        kv_copy(me, kv_send.at[i], chip_of(i)).start()

    kv_copy(me, part_send.at[0], (sp, partner)).start()

    q = mm(normed, wq_ref[...])
    q_rows = pl.ds(pl.multiple_of(tp * rows, 16), rows)
    q_ref[q_rows, :] = (q * rms(q, q.shape[1]) * qg_ref[...].astype(F32)).astype(BF16)

    def q_copy(i):
        return pltpu.make_async_remote_copy(
            src_ref=q_ref.at[q_rows], dst_ref=q_ref.at[q_rows], send_sem=q_send.at[i],
            recv_sem=q_recv.at[i], device_id=(sp, lax.rem(tp + i, n_tp)), device_id_type=MESH)

    for i in range(1, n_tp):
        q_copy(i).start()
    pool = mm(normed, wp_ref[...]).astype(BF16)
    for t in range(n_tp):
        pool_src[t] = pool[:, t * pool_cols : (t + 1) * pool_cols]
    pool_ref[pl.ds(pl.multiple_of(HALO + tp * rows, 16), rows), :] = pool_src[tp]

    def p_copy(i):
        t = lax.rem(tp + i, n_tp)
        return pltpu.make_async_remote_copy(
            src_ref=pool_src.at[t],
            dst_ref=pool_ref.at[pl.ds(pl.multiple_of(HALO + tp * rows, 16), rows)],
            send_sem=p_send.at[i], recv_sem=p_recv.at[i],
            device_id=(sp, t), device_id_type=MESH)

    for i in range(1, n_tp):
        p_copy(i).start()
    last = HALO + n_tp * rows

    def up_copy(t):
        return pltpu.make_async_remote_copy(
            src_ref=pool_src.at[t, pl.ds(rows - HALO, HALO)], dst_ref=pool_ref.at[pl.ds(0, HALO)],
            send_sem=h_send.at[t], recv_sem=h_recv.at[0], device_id=(sp + 1, t), device_id_type=MESH)

    def down_copy(t):
        return pltpu.make_async_remote_copy(
            src_ref=pool_src.at[t, pl.ds(0, HALO)], dst_ref=pool_ref.at[pl.ds(last, HALO)],
            send_sem=h_send.at[n_tp + t], recv_sem=h_recv.at[1], device_id=(sp - 1, t), device_id_type=MESH)

    sends_up = jnp.logical_and(tp == n_tp - 1, sp < n_sp - 1)
    sends_down = jnp.logical_and(tp == 0, sp > 0)

    @pl.when(sends_up)
    def _():
        for t in range(n_tp):
            up_copy(t).start()

    @pl.when(sends_down)
    def _():
        for t in range(n_tp):
            down_copy(t).start()

    @pl.when(sp == 0)
    def _():
        pool_ref[:HALO, :] = jnp.zeros((HALO, pool_cols), BF16)

    @pl.when(sp == n_sp - 1)
    def _():
        pool_ref[last:, :] = jnp.zeros((HALO, pool_cols), BF16)

    @pl.loop(1, n_chip)
    def _(i):
        slot = source_of(i)
        kv_copy(slot, part_send.at[i], (sp, partner)).wait_recv()
        kv_copy(slot, part_send.at[i], (sp, partner)).start()

    @pl.loop(0, n_chip)
    def _(i):
        slot = source_of(i) - core + 1 - core
        kv_copy(slot, part_send.at[i], (sp, partner)).wait_recv()

    for i in range(1, n_tp):
        q_copy(i).wait()
        p_copy(i).wait()

    @pl.when(sp > 0)
    def _():
        pltpu.make_async_remote_copy(
            src_ref=pool_src.at[0, pl.ds(0, HALO)], dst_ref=pool_ref.at[pl.ds(0, HALO)],
            send_sem=h_send.at[0], recv_sem=h_recv.at[0], device_id=(sp, partner), device_id_type=MESH).wait_recv()

    @pl.when(sp < n_sp - 1)
    def _():
        pltpu.make_async_remote_copy(
            src_ref=pool_src.at[0, pl.ds(0, HALO)], dst_ref=pool_ref.at[pl.ds(last, HALO)],
            send_sem=h_send.at[0], recv_sem=h_recv.at[1], device_id=(sp, partner), device_id_type=MESH).wait_recv()

    @pl.when(sends_up)
    def _():
        for t in range(n_tp):
            up_copy(t).wait_send()

    @pl.when(sends_down)
    def _():
        for t in range(n_tp):
            down_copy(t).wait_send()

    @pl.loop(1, n_chip)
    def _(i):
        kv_copy(me, kv_send.at[i], chip_of(i)).wait_send()

    @pl.loop(0, n_chip)
    def _(i):
        kv_copy(me, part_send.at[i], (sp, partner)).wait_send()


def turn(y, cosine, sine, lane):
    half = ROT // 2
    width = y.shape[-1]
    swapped = jnp.where(lane < PLAIN + half, pltpu.roll(y, width - half, 1), pltpu.roll(y, half, 1))
    return y * cosine + swapped * sine


def mixer_kernel(n_sp, n_tp, q_ref, pool_ref, kv_ref, wqu_ref, wkvu_ref, qg_ref, kg_ref, mix_ref, scale_ref,
                 woa_ref, wop_ref, base_ref, block_ref,
                 out_ref, lse_ref, q_s, k_s, v_s, cat_s):
    sp = lax.axis_index("sp")
    tp = lax.axis_index("tp")
    rows = q_ref.shape[0]
    part = rows // n_tp
    heads = wqu_ref.shape[1] // HEAD
    pairs = q_s.shape[0] // 2
    rank = kv_ref.shape[2]
    lane = lax.broadcasted_iota(jnp.int32, (rows, 128), 1)

    def table(b):
        ca, sa = base_ref[:, :128], base_ref[:, 128:]
        cb, sb = block_ref[b, :, :128], block_ref[b, :, 128:]
        return ca * cb - sa * sb, sa * cb + ca * sb

    cq, sq = table(sp)
    qg = qg_ref[...]
    ql = q_ref[...]
    for h in range(heads):
        w = jnp.concatenate(
            [wqu_ref[:, h * HEAD : (h + 1) * HEAD], jnp.zeros((wqu_ref.shape[0], 128 - HEAD), BF16)], axis=1)
        y = mm(ql, w)
        q_s[h] = turn(y * rms(y, HEAD) * qg, cq, sq, lane).astype(BF16)

    for h in range(heads, 2 * pairs):
        q_s[h] = jnp.zeros(q_s.shape[1:], BF16)

    kg = kg_ref[...]

    @pl.loop(0, n_sp)
    def _(b):
        lat = jnp.concatenate([kv_ref[b * n_tp + t, :part, :] for t in range(n_tp)], axis=0)
        pieces = []
        for t in range(n_tp):
            packed = kv_ref[b * n_tp + t, part:, :].astype(F32)
            for j in range(part // 16):
                pieces.append(packed[:, j * ROT : (j + 1) * ROT])
        rope = jnp.concatenate(pieces, axis=0)
        rope = jnp.concatenate([jnp.zeros((rows, PLAIN), F32), rope, jnp.zeros((rows, 128 - HEAD), F32)], axis=1)
        rope_sum = jnp.sum(rope * rope, axis=-1, keepdims=True)
        ck, sk = table(b)
        rotated = turn(rope * kg, ck, sk, lane)
        pair = mm(lat, wkvu_ref[...])
        at = pl.ds(pl.multiple_of(b * rows, 128), rows)
        for h in range(heads):
            kvh = pair[:, h * 128 : (h + 1) * 128]
            plain = jnp.where(lane < PLAIN, kvh, 0.0)
            r = lax.rsqrt((jnp.sum(plain * plain, axis=-1, keepdims=True) + rope_sum) * (1.0 / HEAD) + EPS)
            k_s[h, at, :] = (jnp.where(lane < PLAIN, kvh * kg, rotated) * r).astype(BF16)
            v_s[h, at, :] = jnp.where(lane < PLAIN, 1.0, kvh).astype(BF16)
        for h in range(heads, 2 * pairs):
            k_s[h, at, :] = jnp.zeros((rows, 128), BF16)
            v_s[h, at, :] = jnp.ones((rows, 128), BF16)

    chunk = 128
    lane_c = lax.broadcasted_iota(jnp.int32, (chunk, 128), 1)

    def one_head(h, at):
        s = lax.dot_general(q_s[h, at, :], k_s[h], (((1,), (1,)), ((), ())), preferred_element_type=F32)
        m = jnp.max(s, axis=-1, keepdims=True)
        p = jnp.exp2(s - m).astype(BF16)
        o = mm(p, v_s[h])
        total = o[:, :1]
        lse = m * np.float32(np.log(2.0)) + jnp.log(total)
        return o * (1.0 / total), lse

    @pl.loop(0, rows // chunk)
    def _(c):
        at = pl.ds(pl.multiple_of(c * chunk, chunk), chunk)

        @pl.loop(0, pairs)
        def _(j):
            even, lse0 = one_head(2 * j, at)
            odd, lse1 = one_head(2 * j + 1, at)
            both = jnp.where(lane_c < VALUE, pltpu.roll(even, VALUE, 1), odd)
            cat_s[j, at, :] = both.astype(BF16)
            two = jnp.concatenate([lse0, lse1], axis=1)
            lse_ref[pl.ds(j, 1), :, at] = jnp.transpose(two)[None]

    x = pool_ref[...].astype(F32)
    size = x.shape[0]
    w1 = x + pltpu.roll(x, 1, 0)
    w2 = pltpu.roll(w1, 1, 0) + pltpu.roll(w1, size - 1, 0)
    w4 = pltpu.roll(w2, 2, 0) + pltpu.roll(w2, size - 2, 0)
    w8 = pltpu.roll(w4, 4, 0) + pltpu.roll(w4, size - 4, 0)
    x, w1, w2, w4, w8 = (v[HALO : HALO + rows] for v in (x, w1, w2, w4, w8))
    groups_here = mix_ref.shape[0]
    wide = x.shape[1]
    kind = lax.rem(tp * groups_here + lane[:, :wide] // GDIM, 4)
    window = jnp.where(kind == 0, w1, jnp.where(kind == 1, w2, jnp.where(kind == 2, w4, w8)))
    half = jnp.where(kind == 0, 1, jnp.where(kind == 1, 2, jnp.where(kind == 2, 4, 8)))
    place = sp * rows + lax.broadcasted_iota(jnp.int32, (rows, wide), 0)
    count = (jnp.minimum(place + half, rows * n_sp) - jnp.maximum(place - half, 0)).astype(F32)
    pooled = (window / count - x).astype(BF16)
    mapped = jnp.concatenate(
        [mm(pooled[:, g * GDIM : (g + 1) * GDIM], mix_ref[g]) for g in range(groups_here)], axis=1)
    pool_out = (mapped * scale_ref[...].astype(F32)).astype(BF16)
    attention = jnp.concatenate([cat_s[j] for j in range(pairs)], axis=1)[:, : heads * VALUE]
    tile = 512

    @pl.loop(0, out_ref.shape[1] // tile)
    def _(i):
        cols = pl.ds(pl.multiple_of(i * tile, tile), tile)
        out_ref[:, cols] = (mm(attention, woa_ref[:, cols]) + mm(pool_out, wop_ref[:, cols])).astype(BF16)


def scatter_kernel(n_tp, pieces, x_ref, out_ref, from_partner, to_send, from_chip, d_send, d_recv, c_send, c_recv):
    sp = lax.axis_index("sp")
    tp = lax.axis_index("tp")
    n_ty = n_tp // 2
    core = lax.rem(tp, 2)
    ty = tp // 2
    partner = ty * 2 + 1 - core
    rows = out_ref.shape[0]
    width = out_ref.shape[1] // pieces
    barrier = pltpu.get_barrier_semaphore()
    for i in range(1, n_tp):
        pl.semaphore_signal(barrier, inc=1, device_id=(sp, lax.rem(tp + i, n_tp)), device_id_type=MESH)
    pl.semaphore_wait(barrier, n_tp - 1)

    def cols(p):
        return pl.ds(p * width, width)

    def at(i, c):
        return pl.ds(pl.multiple_of((lax.rem(ty + i, n_ty) * 2 + c) * rows, 16), rows)

    def d_copy(i, p):
        return pltpu.make_async_remote_copy(
            src_ref=x_ref.at[at(i, 1 - core), cols(p)], dst_ref=from_partner.at[i, :, cols(p)],
            send_sem=d_send.at[i * pieces + p], recv_sem=d_recv.at[i * pieces + p],
            device_id=(sp, partner), device_id_type=MESH)

    def c_copy(i, p):
        return pltpu.make_async_remote_copy(
            src_ref=to_send.at[i, :, cols(p)], dst_ref=from_chip.at[i, :, cols(p)],
            send_sem=c_send.at[i * pieces + p], recv_sem=c_recv.at[i * pieces + p],
            device_id=(sp, lax.rem(ty + i, n_ty) * 2 + core), device_id_type=MESH)

    order = [(i, p) for i in list(range(1, n_ty)) + [0] for p in range(pieces)]
    for i, p in order:
        d_copy(i, p).start()
    for i, p in order:
        if i:
            d_copy(i, p).wait_recv()
            to_send[i, :, cols(p)] = (
                x_ref[at(i, core), cols(p)].astype(F32) + from_partner[i, :, cols(p)].astype(F32)).astype(BF16)
            c_copy(i, p).start()
    for p in range(pieces):
        d_copy(0, p).wait_recv()
        total = x_ref[at(0, core), cols(p)].astype(F32) + from_partner[0, :, cols(p)].astype(F32)
        for i in range(1, n_ty):
            c_copy(i, p).wait_recv()
            total = total + from_chip[i, :, cols(p)].astype(F32)
        out_ref[:, cols(p)] = total.astype(BF16)
    for i, p in order:
        d_copy(i, p).wait_send()
        if i:
            c_copy(i, p).wait_send()


def tables(rows, blocks):
    half = ROT // 2
    freqs = ROPE_BASE ** (-np.arange(half, dtype=np.float64) / half)

    def make(positions):
        angle = positions[:, None] * freqs[None, :]
        out = np.zeros((len(positions), 256), np.float64)
        out[:, :PLAIN] = 1.0
        out[:, PLAIN:HEAD] = np.concatenate([np.cos(angle), np.cos(angle)], axis=1)
        out[:, 128 + PLAIN : 128 + HEAD] = np.concatenate([-np.sin(angle), np.sin(angle)], axis=1)
        return out.astype(np.float32)

    return make(np.arange(rows)), make(np.arange(blocks) * rows)[:, None]


def shards(n_sp, n_tp, tokens, norm_gain, wq, q_lat_gain, wkv, kv_lat_gain, w_rope, w_pool_in, wqu, wkvu,
           query_gain, key_gain, w_mix, pool_scale, w_out_attn, w_out_pool):
    rows_own, width = tokens.shape
    rows = rows_own * n_tp
    heads = wqu.shape[1] // HEAD
    pool_cols = w_mix.shape[0] * GDIM
    n_dev = n_sp * n_tp
    n_chip = n_dev // 2
    dma = pltpu.SemaphoreType.DMA
    rank = wkv.shape[1]
    q_lat, pool_in, kvr = pl.pallas_call(
        functools.partial(gather_kernel, n_sp, n_tp),
        out_shape=[
            jax.ShapeDtypeStruct((rows, wq.shape[1]), BF16),
            jax.ShapeDtypeStruct((rows + 2 * HALO, pool_cols), BF16),
            jax.ShapeDtypeStruct((n_dev, rows_own + 16, rank), BF16),
        ],
        in_specs=[VMEM] * 8,
        out_specs=[VMEM] * 3,
        scratch_shapes=[
            pltpu.VMEM((n_tp, rows_own, pool_cols), BF16),
            dma((n_chip,)), dma((n_dev,)), dma((n_chip,)),
            dma((n_tp,)), dma((n_tp,)), dma((n_tp,)), dma((n_tp,)), dma((2 * n_tp,)), dma((2,)),
        ],
        compiler_params=pltpu.CompilerParams(
            collective_id=0, has_side_effects=True, vmem_limit_bytes=60 * 2**20),
    )(tokens, norm_gain[None], wq, q_lat_gain[None], wkv, kv_lat_gain[None], w_rope, w_pool_in)

    base, block = tables(rows, n_sp)
    pad = (0, 128 - HEAD)
    factor = np.float32(HEAD ** -0.5 * np.log2(np.e))
    qg = jnp.pad(query_gain.astype(F32) * factor, pad)[None]
    kg = jnp.pad(key_gain.astype(F32), pad)[None]
    total = rows * n_sp
    pairs = (heads + 1) // 2
    partial, lse = pl.pallas_call(
        functools.partial(mixer_kernel, n_sp, n_tp),
        out_shape=[
            jax.ShapeDtypeStruct((rows, width), BF16),
            jax.ShapeDtypeStruct((pairs, 2, rows), F32),
        ],
        in_specs=[VMEM] * 13,
        out_specs=[VMEM] * 2,
        scratch_shapes=[
            pltpu.VMEM((2 * pairs, rows, 128), BF16),
            pltpu.VMEM((2 * pairs, total, 128), BF16),
            pltpu.VMEM((2 * pairs, total, 128), BF16),
            pltpu.VMEM((pairs, rows, 128), BF16),
        ],
        compiler_params=pltpu.CompilerParams(vmem_limit_bytes=62 * 2**20),
    )(q_lat, pool_in, kvr, wqu, wkvu, qg, kg, w_mix, pool_scale[None], w_out_attn, w_out_pool, base, block)

    pieces = 2
    n_ty = n_tp // 2
    mixed = pl.pallas_call(
        functools.partial(scatter_kernel, n_tp, pieces),
        out_shape=jax.ShapeDtypeStruct((rows_own, width), BF16),
        in_specs=[VMEM],
        out_specs=VMEM,
        scratch_shapes=[
            pltpu.VMEM((n_ty, rows_own, width), BF16),
            pltpu.VMEM((n_ty, rows_own, width), BF16),
            pltpu.VMEM((n_ty, rows_own, width), BF16),
            dma((n_ty * pieces,)), dma((n_ty * pieces,)), dma((n_ty * pieces,)), dma((n_ty * pieces,)),
        ],
        compiler_params=pltpu.CompilerParams(collective_id=1, has_side_effects=True),
    )(partial)
    return mixed, lse.reshape(2 * pairs, rows)[:heads]


def solution(mesh):
    placed = (
        P(("sp", "tp"), None), P(), P(), P(), P(), P(), P(), P(),
        P(None, "tp"), P(None, "tp"), P(), P(),
        P("tp", None, None), P("tp"), P("tp", None), P("tp", None),
    )
    return jax.shard_map(
        functools.partial(shards, mesh.shape["sp"], mesh.shape["tp"]),
        mesh=mesh,
        in_specs=placed,
        out_specs=(P(("sp", "tp"), None), P("tp", "sp")),
        check_vma=False,
    )
```

time: 177 us -> 90.1 us (0.51)
  the two profiles are of different devices: /device:TPU:0 before, /device:TPU:10 now
where the time goes in v1:
time: 90.1 us; the launch traced here: 89.7 us
  Pallas kernels  76.4 us (85%)
  local copies, waits for them, and re-layouts  10.8 us (12%)
  other arithmetic  1.88 us (2%)
    pallas_call x1, Pallas kernels, shards(): pl.pallas_call(functools.partial(gather_kernel, n_sp, n_tp), out_shape=[j...  32.2 us
    pallas_call x1, Pallas kernels, shards(): pl.pallas_call(functools.partial(mixer_kernel, n_sp, n_tp), out_shape=[ja...  28.9 us
    pallas_call x1, Pallas kernels, shards(): pl.pallas_call(functools.partial(scatter_kernel, n_tp, pieces), out_shape...  15.3 us
    unnamed x5, local copies, waits for them, and re-layouts  5.85 us

profile of v1, /device:TPU:10, one launch (start us, length us, event | category | flops | bytes accessed | tf_op | source)
XLA Modules:
  0.0 89.7 jit_solution(6263963378393289058)
XLA Ops:
  0.6 0.7 convert_multiply_fusion
  1.3 0.5 pad_bitcast_fusion.qg_ref
  1.8 1.2 %bitcast_convert_fusion.kg_ref = f32[1,128]{1,0:T(1,128)} fusion(bf16[96]{0:T(256)(128)(2,1)} %param.29), kind=kLoop, calls=%fused_computation | loop fusion | flops 128 | bytes 704 | tf_op jit(solution)/shard_map/broadcast_in_dim | solution.py:407
  3.0 1.2 %broadcast_in_dim.22.kvg_ref = bf16[1,256]{1,0:T(2,128)(2,1)} reshape(bf16[256]{0:T(256)(128)(2,1)} %param.23) | data formatting | bytes 1024 | tf_op jit(solution)/shard_map/broadcast_in_dim | solution.py:401
  4.3 1.3 %broadcast_in_dim.21.qg_ref = bf16[1,512]{1,0:T(2,128)(2,1)} reshape(bf16[512]{0:T(512)(128)(2,1)} %param.21) | data formatting | bytes 2048 | tf_op jit(solution)/shard_map/broadcast_in_dim | solution.py:401
  5.5 1.3 %broadcast_in_dim.20.gain_ref = bf16[1,2048]{1,0:T(2,128)(2,1)} reshape(bf16[2048]{0:T(1024)(128)(2,1)} %param.19) | data formatting | bytes 8192 | tf_op jit(solution)/shard_map/broadcast_in_dim | solution.py:401
  6.8 1.9 %copy.20.wr_ref = bf16[2048,32]{1,0:T(8,128)(2,1)} copy(bf16[2048,32]{0,1:T(8,128)(2,1)} %param.24) | data formatting | bytes 262144 | tf_op args[6]
  8.7 2.2 %copy.21.wqu_ref = bf16[512,576]{1,0:T(8,128)(2,1)} copy(bf16[512,576]{0,1:T(8,128)(2,1)} %param.26) | data formatting | bytes 1179648 | tf_op args[8]
  10.9 32.2 %shard_map.185 = (bf16[384,512]{1,0:T(8,128)(2,1)}, bf16[416,128]{1,0:T(8,128)(2,1)}, bf16[32,112,256]{2,1,0:T(8,128)(2,1)}) custom-call(bf16[96,2048]{1,0:T(8,128)(2,1)} %x_ref.1, bf16[1,2048]{1,0:T(2,128)(2,1)} %broadcast_in_dim.20.gain_ref, bf16[2048,512]{1,0:T(8,128)(2,1)} %wq_ref.1, bf16[1,512]{1,0:T(2,128)(2,1)} %broadcast_in_dim.21.qg_ref, ...), custom_call_target="tpu_custom_call" | custom-call | tf_op jit(solution)/shard_map/pallas_call | solution.py:385
  43.1 28.9 %shard_map.186 = (bf16[384,2048]{1,0:T(8,128)(2,1)}, f32[3,2,384]{2,1,0:T(2,128)}) custom-call(bf16[384,512]{1,0:T(8,128)(2,1)} %get-tuple-element.7.q_ref, bf16[416,128]{1,0:T(8,128)(2,1)} %get-tuple-element.8.pool_ref, bf16[32,112,256]{2,1,0:T(8,128)(2,1)} %get-tuple-element.9.kv_ref, bf16[512,576]{1,0:T(8,128)(2,1)} %copy.21.wqu_ref, ...), custom_call_target="tpu_custom_call" | custom-call | tf_op jit(solution)/shard_map/pallas_call | solution.py:410
  72.0 0.0 copy-start
  72.0 15.3 %shard_map.187 = bf16[96,2048]{1,0:T(8,128)(2,1)} custom-call(bf16[384,2048]{1,0:T(8,128)(2,1)} %get-tuple-element.10.x_ref), custom_call_target="tpu_custom_call" | custom-call | tf_op jit(solution)/shard_map/pallas_call | solution.py:429
  87.3 0.0 copy-done
  87.4 0.6 reshape.7
  88.0 1.8 %copy.23 = bf16[96,2048]{1,0:T(8,128)(2,1)} copy(bf16[96,2048]{1,0:T(8,128)(2,1)} %shard_map.187) | data formatting | bytes 786432
Async XLA Ops:
  72.0 15.4 %copy-start = (f32[3,2,384]{2,1,0:T(2,128)S(1)}, f32[3,2,384]{2,1,0:T(2,128)}, u32[]{:S(2)}) copy-start(f32[3,2,384]{2,1,0:T(2,128)} %get-tuple-element.11) | copy-start | bytes 27652

commit v2 on v1

v2 whole, which is shorter than its diff:
```python
import functools

import jax
import jax.numpy as jnp
import numpy as np
from jax import lax
from jax.experimental import pallas as pl
from jax.experimental.pallas import tpu as pltpu
from jax.sharding import PartitionSpec as P

PLAIN = 64
ROT = 32
HEAD = PLAIN + ROT
VALUE = 64
GDIM = 64
EPS = 1e-06
ROPE_BASE = 10000.0
HALO = 16
F32 = jnp.float32
BF16 = jnp.bfloat16
MESH = pl.DeviceIdType.MESH
VMEM = pl.BlockSpec(memory_space=pltpu.VMEM)


def rms(x, width):
    return lax.rsqrt(jnp.sum(x * x, axis=-1, keepdims=True) * (1.0 / width) + EPS)


def row(ref, width=None):
    v = ref[...].astype(F32).reshape(1, ref.shape[0])
    if width and width > ref.shape[0]:
        v = jnp.concatenate([v, jnp.zeros((1, width - ref.shape[0]), F32)], axis=1)
    return v


def mm_t(a, b):
    return lax.dot_general(a, b, (((1,), (1,)), ((), ())), preferred_element_type=F32)


def mm(a, b):
    return jnp.dot(a, b, preferred_element_type=F32)


def turn(y, cosine, sine, lane):
    half = ROT // 2
    width = y.shape[-1]
    swapped = jnp.where(lane < PLAIN + half, pltpu.roll(y, width - half, 1), pltpu.roll(y, half, 1))
    return y * cosine + swapped * sine


def layer_kernel(n_sp, n_tp, pieces, x_ref, gain_ref, wq_ref, qlg_ref, wkv_ref, kvg_ref, wr_ref, wp_ref,
                 wqu_ref, wkvu_ref, qg_ref, kg_ref, mix_ref, scale_ref, woa_ref, wop_ref, base_ref, block_ref,
                 out_ref, lse_ref,
                 q_ref, pool_ref, kv_ref, pool_src, q_s, k_s, v_s, cat_s, att_s, part_s, from_partner, to_send, from_chip,
                 kv_send, kv_recv, part_send, q_send, q_recv, p_send, p_recv, h_send, h_recv,
                 d_send, d_recv, c_send, c_recv):
    sp = lax.axis_index("sp")
    tp = lax.axis_index("tp")
    n_dev = n_sp * n_tp
    n_ty = n_tp // 2
    n_chip = n_sp * n_ty
    me = sp * n_tp + tp
    core = lax.rem(tp, 2)
    ty = tp // 2
    partner = ty * 2 + 1 - core
    part = x_ref.shape[0]
    pool_cols = pool_ref.shape[1]
    barrier = pltpu.get_barrier_semaphore()

    @pl.loop(1, n_dev)
    def _(i):
        d = lax.rem(me + i, n_dev)
        pl.semaphore_signal(barrier, inc=1, device_id=(d // n_tp, lax.rem(d, n_tp)), device_id_type=MESH)

    x = x_ref[...].astype(F32)
    normed = (x * rms(x, x.shape[1]) * row(gain_ref)).astype(BF16)
    kv = mm(normed, wkv_ref[...])
    kv_ref[me, :part, :] = (kv * rms(kv, kv.shape[1]) * row(kvg_ref)).astype(BF16)
    rope = mm_t(normed, wr_ref[...])
    groups = part // 16
    packed = [rope[16 * j : 16 * j + 16, :] for j in range(groups)]
    packed.append(jnp.zeros((16, kv.shape[1] - groups * ROT), F32))
    kv_ref[me, part:, :] = jnp.concatenate(packed, axis=1).astype(BF16)
    pl.semaphore_wait(barrier, n_dev - 1)

    def chip_of(i):
        s = lax.rem(sp + i // n_ty, n_sp)
        t = lax.rem(ty + lax.rem(i, n_ty), n_ty) * 2 + core
        return s, t

    def source_of(i):
        s = lax.rem(sp + n_sp - i // n_ty, n_sp)
        t = lax.rem(ty + n_ty - lax.rem(i, n_ty), n_ty) * 2 + core
        return s * n_tp + t

    def kv_copy(slot, send_sem, target):
        return pltpu.make_async_remote_copy(
            src_ref=kv_ref.at[slot], dst_ref=kv_ref.at[slot], send_sem=send_sem,
            recv_sem=kv_recv.at[slot], device_id=target, device_id_type=MESH)

    @pl.loop(1, n_chip)
    def _(i):
        kv_copy(me, kv_send.at[i], chip_of(i)).start()

    kv_copy(me, part_send.at[0], (sp, partner)).start()

    q = mm(normed, wq_ref[...])
    q_rows = pl.ds(pl.multiple_of(tp * part, 16), part)
    q_ref[q_rows, :] = (q * rms(q, q.shape[1]) * row(qlg_ref)).astype(BF16)

    def q_copy(i):
        return pltpu.make_async_remote_copy(
            src_ref=q_ref.at[q_rows], dst_ref=q_ref.at[q_rows], send_sem=q_send.at[i],
            recv_sem=q_recv.at[i], device_id=(sp, lax.rem(tp + i, n_tp)), device_id_type=MESH)

    for i in range(1, n_tp):
        q_copy(i).start()
    pool = mm(normed, wp_ref[...]).astype(BF16)
    for t in range(n_tp):
        pool_src[t] = pool[:, t * pool_cols : (t + 1) * pool_cols]
    pool_ref[pl.ds(pl.multiple_of(HALO + tp * part, 16), part), :] = pool_src[tp]

    def p_copy(i):
        t = lax.rem(tp + i, n_tp)
        return pltpu.make_async_remote_copy(
            src_ref=pool_src.at[t],
            dst_ref=pool_ref.at[pl.ds(pl.multiple_of(HALO + tp * part, 16), part)],
            send_sem=p_send.at[i], recv_sem=p_recv.at[i],
            device_id=(sp, t), device_id_type=MESH)

    for i in range(1, n_tp):
        p_copy(i).start()
    last = HALO + n_tp * part

    def up_copy(t):
        return pltpu.make_async_remote_copy(
            src_ref=pool_src.at[t, pl.ds(part - HALO, HALO)], dst_ref=pool_ref.at[pl.ds(0, HALO)],
            send_sem=h_send.at[t], recv_sem=h_recv.at[0], device_id=(sp + 1, t), device_id_type=MESH)

    def down_copy(t):
        return pltpu.make_async_remote_copy(
            src_ref=pool_src.at[t, pl.ds(0, HALO)], dst_ref=pool_ref.at[pl.ds(last, HALO)],
            send_sem=h_send.at[n_tp + t], recv_sem=h_recv.at[1], device_id=(sp - 1, t), device_id_type=MESH)

    sends_up = jnp.logical_and(tp == n_tp - 1, sp < n_sp - 1)
    sends_down = jnp.logical_and(tp == 0, sp > 0)

    @pl.when(sends_up)
    def _():
        for t in range(n_tp):
            up_copy(t).start()

    @pl.when(sends_down)
    def _():
        for t in range(n_tp):
            down_copy(t).start()

    @pl.when(sp == 0)
    def _():
        pool_ref[:HALO, :] = jnp.zeros((HALO, pool_cols), BF16)

    @pl.when(sp == n_sp - 1)
    def _():
        pool_ref[last:, :] = jnp.zeros((HALO, pool_cols), BF16)


    rows = n_tp * part
    heads = wqu_ref.shape[0] // HEAD
    pairs = q_s.shape[0] // 2
    lane = lax.broadcasted_iota(jnp.int32, (rows, 128), 1)

    def table(b):
        ca, sa = base_ref[:, :128], base_ref[:, 128:]
        cb, sb = block_ref[b, :, :128], block_ref[b, :, 128:]
        return ca * cb - sa * sb, sa * cb + ca * sb

    def relay(k):
        @pl.loop(0, n_ty)
        def _(j):
            i = k * n_ty + j

            @pl.when(i > 0)
            def _():
                slot = source_of(i)
                kv_copy(slot, part_send.at[i], (sp, partner)).wait_recv()
                kv_copy(slot, part_send.at[i], (sp, partner)).start()

    kg = row(kg_ref, 128)

    def build_keys(k):
        @pl.loop(0, n_ty)
        def _(j):
            i = k * n_ty + j
            slot = source_of(i) - core + 1 - core
            kv_copy(slot, part_send.at[i], (sp, partner)).wait_recv()

        b = lax.rem(sp + n_sp - k, n_sp)
        lat = jnp.concatenate([kv_ref[b * n_tp + t, :part, :] for t in range(n_tp)], axis=0)
        parts = []
        for t in range(n_tp):
            packed = kv_ref[b * n_tp + t, part:, :].astype(F32)
            for j in range(part // 16):
                parts.append(packed[:, j * ROT : (j + 1) * ROT])
        rope = jnp.concatenate(parts, axis=0)
        rope = jnp.concatenate([jnp.zeros((rows, PLAIN), F32), rope, jnp.zeros((rows, 128 - HEAD), F32)], axis=1)
        rope_sum = jnp.sum(rope * rope, axis=-1, keepdims=True)
        ck, sk = table(b)
        rotated = turn(rope * kg, ck, sk, lane)
        pair = mm(lat, wkvu_ref[...])
        at = pl.ds(pl.multiple_of(b * rows, 128), rows)
        for h in range(heads):
            kvh = pair[:, h * 128 : (h + 1) * 128]
            plain = jnp.where(lane < PLAIN, kvh, 0.0)
            r = lax.rsqrt((jnp.sum(plain * plain, axis=-1, keepdims=True) + rope_sum) * (1.0 / HEAD) + EPS)
            k_s[h, at, :] = (jnp.where(lane < PLAIN, kvh * kg, rotated) * r).astype(BF16)
            v_s[h, at, :] = jnp.where(lane < PLAIN, 1.0, kvh).astype(BF16)
        for h in range(heads, 2 * pairs):
            k_s[h, at, :] = jnp.zeros((rows, 128), BF16)
            v_s[h, at, :] = jnp.ones((rows, 128), BF16)

    relay(0)
    for i in range(1, n_tp):
        q_copy(i).wait_recv()
    cq, sq = table(sp)
    qg = row(qg_ref, 128) * np.float32(HEAD ** -0.5 * np.log2(np.e))
    ql = q_ref[...]
    for h in range(heads):
        w = jnp.concatenate(
            [wqu_ref[h * HEAD : (h + 1) * HEAD, :], jnp.zeros((128 - HEAD, wqu_ref.shape[1]), BF16)], axis=0)
        y = mm_t(ql, w)
        q_s[h] = turn(y * rms(y, HEAD) * qg, cq, sq, lane).astype(BF16)
    for h in range(heads, 2 * pairs):
        q_s[h] = jnp.zeros(q_s.shape[1:], BF16)

    @pl.loop(0, n_sp)
    def _(k):
        @pl.when(k < n_sp - 1)
        def _():
            relay(k + 1)

        build_keys(k)

    for i in range(1, n_tp):
        p_copy(i).wait_recv()

    def halo_wait(start, side):
        pltpu.make_async_remote_copy(
            src_ref=pool_src.at[0, pl.ds(0, HALO)], dst_ref=pool_ref.at[pl.ds(start, HALO)],
            send_sem=h_send.at[0], recv_sem=h_recv.at[side], device_id=(sp, partner),
            device_id_type=MESH).wait_recv()

    @pl.when(sp > 0)
    def _():
        halo_wait(0, 0)

    @pl.when(sp < n_sp - 1)
    def _():
        halo_wait(last, 1)

    x = pool_ref[...].astype(F32)
    size = x.shape[0]
    w1 = x + pltpu.roll(x, 1, 0)
    w2 = pltpu.roll(w1, 1, 0) + pltpu.roll(w1, size - 1, 0)
    w4 = pltpu.roll(w2, 2, 0) + pltpu.roll(w2, size - 2, 0)
    w8 = pltpu.roll(w4, 4, 0) + pltpu.roll(w4, size - 4, 0)
    x, w1, w2, w4, w8 = (v[HALO : HALO + rows] for v in (x, w1, w2, w4, w8))
    groups_here = mix_ref.shape[0]
    wide = x.shape[1]
    kind = lax.rem(tp * groups_here + lane[:, :wide] // GDIM, 4)
    window = jnp.where(kind == 0, w1, jnp.where(kind == 1, w2, jnp.where(kind == 2, w4, w8)))
    half = jnp.where(kind == 0, 1, jnp.where(kind == 1, 2, jnp.where(kind == 2, 4, 8)))
    place = sp * rows + lax.broadcasted_iota(jnp.int32, (rows, wide), 0)
    count = (jnp.minimum(place + half, rows * n_sp) - jnp.maximum(place - half, 0)).astype(F32)
    pooled = (window / count - x).astype(BF16)
    mapped = jnp.concatenate(
        [mm(pooled[:, g * GDIM : (g + 1) * GDIM], mix_ref[g]) for g in range(groups_here)], axis=1)
    cat_s[...] = (mapped * row(scale_ref)).astype(BF16)

    chunk = 2 * part
    lane_c = lax.broadcasted_iota(jnp.int32, (chunk, 128), 1)
    tile = 512
    width = out_ref.shape[1]
    span = width // pieces

    def cols(p):
        return pl.ds(p * span, span)

    def one_head(h, at):
        s = mm_t(q_s[h, at, :], k_s[h])
        m = jnp.max(s, axis=-1, keepdims=True)
        p = jnp.exp2(s - m).astype(BF16)
        o = mm(p, v_s[h])
        total = o[:, :1]
        lse = m * np.float32(np.log(2.0)) + jnp.log(total)
        return o * (1.0 / total), lse

    def d_copy(i, p):
        return pltpu.make_async_remote_copy(
            src_ref=part_s.at[i, 1 - core, :, cols(p)], dst_ref=from_partner.at[i, :, cols(p)],
            send_sem=d_send.at[i * pieces + p], recv_sem=d_recv.at[i * pieces + p],
            device_id=(sp, partner), device_id_type=MESH)

    def c_copy(i, p):
        return pltpu.make_async_remote_copy(
            src_ref=to_send.at[i, :, cols(p)], dst_ref=from_chip.at[i, :, cols(p)],
            send_sem=c_send.at[i * pieces + p], recv_sem=c_recv.at[i * pieces + p],
            device_id=(sp, lax.rem(ty + i, n_ty) * 2 + core), device_id_type=MESH)

    @pl.loop(0, n_ty * pairs)
    def _(step):
        turn_no = step // pairs
        j = lax.rem(step, pairs)
        i = lax.rem(turn_no + 1, n_ty)
        at = pl.ds(pl.multiple_of(lax.rem(ty + i, n_ty) * chunk, 32), chunk)
        even, lse0 = one_head(2 * j, at)
        odd, lse1 = one_head(2 * j + 1, at)
        both = jnp.where(lane_c < VALUE, pltpu.roll(even, VALUE, 1), odd).astype(BF16)
        att_s[j, :, :] = both
        lse_ref[pl.ds(j, 1), pl.ds(lax.rem(ty + i, n_ty), 1), :, :] = jnp.transpose(
            jnp.concatenate([lse0, lse1], axis=1))[None, None]

        @pl.when(jnp.logical_and(j == 0, turn_no > 0))
        def _():
            for p in range(pieces):
                d_copy(turn_no, p).wait_recv()
                to_send[turn_no, :, cols(p)] = (
                    part_s[turn_no, core, :, cols(p)].astype(F32)
                    + from_partner[turn_no, :, cols(p)].astype(F32)).astype(BF16)
                c_copy(turn_no, p).start()

        @pl.when(j == pairs - 1)
        def _():
            attention = jnp.concatenate([att_s[p] for p in range(pairs)], axis=1)[:, : heads * VALUE]
            pool_out = cat_s[at, :]

            for p in range(pieces):
                for n in range(span // tile):
                    cc = pl.ds(p * span + n * tile, tile)
                    y = (mm(attention, woa_ref[:, cc]) + mm(pool_out, wop_ref[:, cc])).astype(BF16)
                    part_s[i, :, :, cc] = y.reshape(2, part, tile)
                d_copy(i, p).start()

    for p in range(pieces):
        d_copy(0, p).wait_recv()
        total = part_s[0, core, :, cols(p)].astype(F32) + from_partner[0, :, cols(p)].astype(F32)
        for i in range(1, n_ty):
            c_copy(i, p).wait_recv()
            total = total + from_chip[i, :, cols(p)].astype(F32)
        out_ref[:, cols(p)] = total.astype(BF16)

    for i in range(n_ty):
        for p in range(pieces):
            d_copy(i, p).wait_send()
            if i:
                c_copy(i, p).wait_send()
    for i in range(1, n_tp):
        q_copy(i).wait_send()
        p_copy(i).wait_send()

    @pl.when(sends_up)
    def _():
        for t in range(n_tp):
            up_copy(t).wait_send()

    @pl.when(sends_down)
    def _():
        for t in range(n_tp):
            down_copy(t).wait_send()

    @pl.loop(1, n_chip)
    def _(i):
        kv_copy(me, kv_send.at[i], chip_of(i)).wait_send()

    @pl.loop(0, n_chip)
    def _(i):
        kv_copy(me, part_send.at[i], (sp, partner)).wait_send()


def tables(rows, blocks):
    half = ROT // 2
    freqs = ROPE_BASE ** (-np.arange(half, dtype=np.float64) / half)

    def make(positions):
        angle = positions[:, None] * freqs[None, :]
        out = np.zeros((len(positions), 256), np.float64)
        out[:, :PLAIN] = 1.0
        out[:, PLAIN:HEAD] = np.concatenate([np.cos(angle), np.cos(angle)], axis=1)
        out[:, 128 + PLAIN : 128 + HEAD] = np.concatenate([-np.sin(angle), np.sin(angle)], axis=1)
        return out.astype(np.float32)

    return make(np.arange(rows)), make(np.arange(blocks) * rows)[:, None]


def shards(n_sp, n_tp, tokens, norm_gain, wq, q_lat_gain, wkv, kv_lat_gain, w_rope, w_pool_in, wqu, wkvu,
           query_gain, key_gain, w_mix, pool_scale, w_out_attn, w_out_pool):
    part, width = tokens.shape
    rows = part * n_tp
    total = rows * n_sp
    heads = wqu.shape[1] // HEAD
    pairs = (heads + 1) // 2
    pool_cols = w_mix.shape[0] * GDIM
    n_dev = n_sp * n_tp
    n_ty = n_tp // 2
    n_chip = n_dev // 2
    pieces = 2
    dma = pltpu.SemaphoreType.DMA
    rank = wkv.shape[1]
    base, block = tables(rows, n_sp)
    mixed, lse = pl.pallas_call(
        functools.partial(layer_kernel, n_sp, n_tp, pieces),
        out_shape=[
            jax.ShapeDtypeStruct((part, width), BF16),
            jax.ShapeDtypeStruct((pairs, n_ty, 2, 2 * part), F32),
        ],
        in_specs=[VMEM] * 18,
        out_specs=[VMEM] * 2,
        scratch_shapes=[
            pltpu.VMEM((rows, wq.shape[1]), BF16),
            pltpu.VMEM((rows + 2 * HALO, pool_cols), BF16),
            pltpu.VMEM((n_dev, part + 16, rank), BF16),
            pltpu.VMEM((n_tp, part, pool_cols), BF16),
            pltpu.VMEM((2 * pairs, rows, 128), BF16),
            pltpu.VMEM((2 * pairs, total, 128), BF16),
            pltpu.VMEM((2 * pairs, total, 128), BF16),
            pltpu.VMEM((rows, pool_cols), BF16),
            pltpu.VMEM((pairs, 2 * part, 128), BF16),
            pltpu.VMEM((n_ty, 2, part, width), BF16),
            pltpu.VMEM((n_ty, part, width), BF16),
            pltpu.VMEM((n_ty, part, width), BF16),
            pltpu.VMEM((n_ty, part, width), BF16),
            dma((n_chip,)), dma((n_dev,)), dma((n_chip,)),
            dma((n_tp,)), dma((n_tp,)), dma((n_tp,)), dma((n_tp,)), dma((2 * n_tp,)), dma((2,)),
            dma((n_ty * pieces,)), dma((n_ty * pieces,)), dma((n_ty * pieces,)), dma((n_ty * pieces,)),
        ],
        compiler_params=pltpu.CompilerParams(
            collective_id=0, has_side_effects=True, vmem_limit_bytes=63 * 2**20),
    )(tokens, norm_gain, wq, q_lat_gain, wkv, kv_lat_gain, w_rope.T, w_pool_in,
      wqu.T, wkvu, query_gain, key_gain, w_mix, pool_scale, w_out_attn, w_out_pool, base, block)
    return mixed, jnp.transpose(lse, (0, 2, 1, 3)).reshape(2 * pairs, rows)[:heads]


def solution(mesh):
    placed = (
        P(("sp", "tp"), None), P(), P(), P(), P(), P(), P(), P(),
        P(None, "tp"), P(None, "tp"), P(), P(),
        P("tp", None, None), P("tp"), P("tp", None), P("tp", None),
    )
    return jax.shard_map(
        functools.partial(shards, mesh.shape["sp"], mesh.shape["tp"]),
        mesh=mesh,
        in_specs=placed,
        out_specs=(P(("sp", "tp"), None), P("tp", "sp")),
        check_vma=False,
    )
```

time: 90.1 us -> 63.4 us (0.70)
  the two profiles are of different devices: /device:TPU:10 before, /device:TPU:0 now
where the time goes in v2:
time: 63.4 us; the launch traced here: 63.2 us
  Pallas kernels  59.4 us (94%)
  local copies, waits for them, and re-layouts  3.16 us (5%)
  between operations  0.65 us (1%)
    pallas_call x1, Pallas kernels, shards(): pl.pallas_call(functools.partial(layer_kernel, n_sp, n_tp, pieces), out_s...  59.4 us
    unnamed x1, local copies, waits for them, and re-layouts  1.77 us

profile of v2, /device:TPU:0, one launch (start us, length us, event | category | flops | bytes accessed | tf_op | source)
XLA Modules:
  0.0 63.2 jit_solution(14062497581929842249)
XLA Ops:
  0.6 59.4 %shard_map.185 = (bf16[96,2048]{1,0:T(8,128)(2,1)}, f32[3,2,2,192]{3,2,1,0:T(2,128)}) custom-call(bf16[96,2048]{1,0:T(8,128)(2,1)} %x_ref.1, bf16[2048]{0:T(1024)(128)(2,1)} %gain_ref.1, bf16[2048,512]{1,0:T(8,128)(2,1)} %wq_ref.1, bf16[512]{0:T(512)(128)(2,1)} %qlg_ref.1, bf16[2048,256]{1,0:T(8,128)(2,1)} %wkv_ref.1, bf16[256]{0:T(256)(128)(2,1)} %kvg_ref.1, ...), custom_call_target="tpu_custom_call" | custom-call | tf_op jit(solution)/shard_map/pallas_call | solution.py:409
  60.0 0.7 %copy.20 = f32[3,2,2,192]{3,2,1,0:T(2,128)S(1)} copy(f32[3,2,2,192]{3,1,2,0:T(2,128)} %bitcast.5) | data formatting | bytes 18432 | tf_op jit(solution)/shard_map/transpose | solution.py:439
  60.7 0.7 %reshape.7 = f32[6,384]{1,0:T(8,128)} reshape(f32[3,2,2,192]{3,2,1,0:T(2,128)S(1)} %copy.20) | data formatting | bytes 18432 | tf_op jit(solution)/shard_map/reshape | solution.py:439
  61.4 1.8 %copy.22 = bf16[96,2048]{1,0:T(8,128)(2,1)} copy(bf16[96,2048]{1,0:T(8,128)(2,1)} %get-tuple-element.8) | data formatting | bytes 786432

commit v3 on v2

--- a/solution.py
+++ b/solution.py
@@ -48,23 +48,33 @@
     return y * cosine + swapped * sine
 
 
-def layer_kernel(n_sp, n_tp, pieces, x_ref, gain_ref, wq_ref, qlg_ref, wkv_ref, kvg_ref, wr_ref, wp_ref,
-                 wqu_ref, wkvu_ref, qg_ref, kg_ref, mix_ref, scale_ref, woa_ref, wop_ref, base_ref, block_ref,
+def layer_kernel(n_sp, n_tp, n_x, pieces, x_ref, gain_ref, wq_hbm, qlg_ref, wkv_ref, kvg_ref, wr_ref, wp_hbm,
+                 wqu_hbm, wkvu_hbm, qg_ref, kg_ref, mix_ref, scale_ref, woa_hbm, wop_hbm, base_ref, block_ref,
                  out_ref, lse_ref,
+                 wq_ref, wp_ref, wqu_ref, wkvu_ref, woa_ref, wop_ref, w_sem,
                  q_ref, pool_ref, kv_ref, pool_src, q_s, k_s, v_s, cat_s, att_s, part_s, from_partner, to_send, from_chip,
-                 kv_send, kv_recv, part_send, q_send, q_recv, p_send, p_recv, h_send, h_recv,
+                 z_send, y_send, x_send, kv_recv, part_send, q_send, q_recv, p_send, p_recv, h_send, h_recv,
                  d_send, d_recv, c_send, c_recv):
     sp = lax.axis_index("sp")
     tp = lax.axis_index("tp")
     n_dev = n_sp * n_tp
     n_ty = n_tp // 2
     n_chip = n_sp * n_ty
+    n_z = n_sp // n_x
     me = sp * n_tp + tp
     core = lax.rem(tp, 2)
     ty = tp // 2
     partner = ty * 2 + 1 - core
     part = x_ref.shape[0]
     pool_cols = pool_ref.shape[1]
+    loads = [
+        pltpu.make_async_copy(source, target, w_sem.at[n])
+        for n, (source, target) in enumerate([
+            (wq_hbm, wq_ref), (wp_hbm, wp_ref), (wqu_hbm, wqu_ref),
+            (wkvu_hbm, wkvu_ref), (woa_hbm, woa_ref), (wop_hbm, wop_ref)])
+    ]
+    for load in loads:
+        load.start()
     barrier = pltpu.get_barrier_semaphore()
 
     @pl.loop(1, n_dev)
@@ -83,27 +93,54 @@
     kv_ref[me, part:, :] = jnp.concatenate(packed, axis=1).astype(BF16)
     pl.semaphore_wait(barrier, n_dev - 1)
 
-    def chip_of(i):
-        s = lax.rem(sp + i // n_ty, n_sp)
-        t = lax.rem(ty + lax.rem(i, n_ty), n_ty) * 2 + core
-        return s, t
-
-    def source_of(i):
-        s = lax.rem(sp + n_sp - i // n_ty, n_sp)
-        t = lax.rem(ty + n_ty - lax.rem(i, n_ty), n_ty) * 2 + core
-        return s * n_tp + t
+    x_of, z_of = lax.rem(sp, n_x), sp // n_x
+
+    def block_of(dx, dz):
+        return lax.rem(z_of + n_z - dz, n_z) * n_x + lax.rem(x_of + n_x - dx, n_x)
+
+    def slot_of(dx, dy, dz):
+        return block_of(dx, dz) * n_tp + lax.rem(ty + n_ty - dy, n_ty) * 2 + core
 
     def kv_copy(slot, send_sem, target):
         return pltpu.make_async_remote_copy(
             src_ref=kv_ref.at[slot], dst_ref=kv_ref.at[slot], send_sem=send_sem,
             recv_sem=kv_recv.at[slot], device_id=target, device_id_type=MESH)
 
-    @pl.loop(1, n_chip)
-    def _(i):
-        kv_copy(me, kv_send.at[i], chip_of(i)).start()
-
-    kv_copy(me, part_send.at[0], (sp, partner)).start()
-
+    def z_copy(i):
+        return kv_copy(me, z_send.at[i], (lax.rem(z_of + i, n_z) * n_x + x_of, tp))
+
+    def y_copy(slot, dz, i):
+        return kv_copy(slot, y_send.at[dz * n_ty + i], (sp, lax.rem(ty + i, n_ty) * 2 + core))
+
+    def x_copy(slot, dy, dz, i):
+        return kv_copy(slot, x_send.at[(dz * n_ty + dy) * n_x + i], (z_of * n_x + lax.rem(x_of + i, n_x), tp))
+
+    def to_partner(slot, dx, dy, dz):
+        return kv_copy(slot, part_send.at[(dx * n_z + dz) * n_ty + dy], (sp, partner))
+
+    def spread(dy, dz):
+        slot = slot_of(0, dy, dz)
+
+        @pl.when(dy + dz > 0)
+        def _():
+            z_wait(slot)
+
+        if isinstance(dy, int):
+            for i in range(1, n_ty):
+                y_copy(slot, dz, i).start()
+        for i in range(1, n_x):
+            x_copy(slot, dy, dz, i).start()
+        to_partner(slot, 0, dy, dz).start()
+
+    def z_wait(slot):
+        kv_copy(slot, part_send.at[0], (sp, partner)).wait_recv()
+
+    for i in range(1, n_z):
+        z_copy(i).start()
+
+    spread(0, jnp.int32(0))
+
+    loads[0].wait()
     q = mm(normed, wq_ref[...])
     q_rows = pl.ds(pl.multiple_of(tp * part, 16), part)
     q_ref[q_rows, :] = (q * rms(q, q.shape[1]) * row(qlg_ref)).astype(BF16)
@@ -115,6 +152,7 @@
 
     for i in range(1, n_tp):
         q_copy(i).start()
+    loads[1].wait()
     pool = mm(normed, wp_ref[...]).astype(BF16)
     for t in range(n_tp):
         pool_src[t] = pool[:, t * pool_cols : (t + 1) * pool_cols]
@@ -176,25 +214,19 @@
 
     def relay(k):
         @pl.loop(0, n_ty)
-        def _(j):
-            i = k * n_ty + j
-
-            @pl.when(i > 0)
-            def _():
-                slot = source_of(i)
-                kv_copy(slot, part_send.at[i], (sp, partner)).wait_recv()
-                kv_copy(slot, part_send.at[i], (sp, partner)).start()
+        def _(dy):
+            slot = slot_of(k // n_z, dy, lax.rem(k, n_z))
+            z_wait(slot)
+            to_partner(slot, k // n_z, dy, lax.rem(k, n_z)).start()
 
     kg = row(kg_ref, 128)
 
     def build_keys(k):
         @pl.loop(0, n_ty)
         def _(j):
-            i = k * n_ty + j
-            slot = source_of(i) - core + 1 - core
-            kv_copy(slot, part_send.at[i], (sp, partner)).wait_recv()
-
-        b = lax.rem(sp + n_sp - k, n_sp)
+            z_wait(slot_of(k // n_z, j, lax.rem(k, n_z)) - core + 1 - core)
+
+        b = block_of(k // n_z, lax.rem(k, n_z))
         lat = jnp.concatenate([kv_ref[b * n_tp + t, :part, :] for t in range(n_tp)], axis=0)
         parts = []
         for t in range(n_tp):
@@ -218,9 +250,14 @@
             k_s[h, at, :] = jnp.zeros((rows, 128), BF16)
             v_s[h, at, :] = jnp.ones((rows, 128), BF16)
 
-    relay(0)
+    @pl.loop(1, n_z)
+    def _(dz):
+        spread(0, dz)
+
     for i in range(1, n_tp):
         q_copy(i).wait_recv()
+    for load in loads[2:]:
+        load.wait()
     cq, sq = table(sp)
     qg = row(qg_ref, 128) * np.float32(HEAD ** -0.5 * np.log2(np.e))
     ql = q_ref[...]
@@ -232,9 +269,13 @@
     for h in range(heads, 2 * pairs):
         q_s[h] = jnp.zeros(q_s.shape[1:], BF16)
 
+    @pl.loop(0, n_z * (n_ty - 1))
+    def _(i):
+        spread(1 + i // n_z, lax.rem(i, n_z))
+
     @pl.loop(0, n_sp)
     def _(k):
-        @pl.when(k < n_sp - 1)
+        @pl.when(jnp.logical_and(k + 1 >= n_z, k < n_sp - 1))
         def _():
             relay(k + 1)
 
@@ -285,9 +326,7 @@
     def cols(p):
         return pl.ds(p * span, span)
 
-    def one_head(h, at):
-        s = mm_t(q_s[h, at, :], k_s[h])
-        m = jnp.max(s, axis=-1, keepdims=True)
+    def finish(s, m, h):
         p = jnp.exp2(s - m).astype(BF16)
         o = mm(p, v_s[h])
         total = o[:, :1]
@@ -312,8 +351,12 @@
         j = lax.rem(step, pairs)
         i = lax.rem(turn_no + 1, n_ty)
         at = pl.ds(pl.multiple_of(lax.rem(ty + i, n_ty) * chunk, 32), chunk)
-        even, lse0 = one_head(2 * j, at)
-        odd, lse1 = one_head(2 * j + 1, at)
+        s0 = mm_t(q_s[2 * j, at, :], k_s[2 * j])
+        m0 = jnp.max(s0, axis=-1, keepdims=True)
+        s1 = mm_t(q_s[2 * j + 1, at, :], k_s[2 * j + 1])
+        m1 = jnp.max(s1, axis=-1, keepdims=True)
+        even, lse0 = finish(s0, m0, 2 * j)
+        odd, lse1 = finish(s1, m1, 2 * j + 1)
         both = jnp.where(lane_c < VALUE, pltpu.roll(even, VALUE, 1), odd).astype(BF16)
         att_s[j, :, :] = both
         lse_ref[pl.ds(j, 1), pl.ds(lax.rem(ty + i, n_ty), 1), :, :] = jnp.transpose(
@@ -367,9 +410,18 @@
         for t in range(n_tp):
             down_copy(t).wait_send()
 
-    @pl.loop(1, n_chip)
-    def _(i):
-        kv_copy(me, kv_send.at[i], chip_of(i)).wait_send()
+    for i in range(1, n_z):
+        z_copy(i).wait_send()
+
+    @pl.loop(0, n_z)
+    def _(dz):
+        for i in range(1, n_ty):
+            y_copy(me, dz, i).wait_send()
+
+        @pl.loop(0, n_ty)
+        def _(dy):
+            for i in range(1, n_x):
+                x_copy(me, dy, dz, i).wait_send()
 
     @pl.loop(0, n_chip)
     def _(i):
@@ -402,19 +454,29 @@
     n_dev = n_sp * n_tp
     n_ty = n_tp // 2
     n_chip = n_dev // 2
+    n_x = 2 ** ((n_sp.bit_length() - 1) // 2)
+    n_x = n_x if n_sp % n_x == 0 else 1
+    n_z = n_sp // n_x
     pieces = 2
     dma = pltpu.SemaphoreType.DMA
     rank = wkv.shape[1]
     base, block = tables(rows, n_sp)
     mixed, lse = pl.pallas_call(
-        functools.partial(layer_kernel, n_sp, n_tp, pieces),
+        functools.partial(layer_kernel, n_sp, n_tp, n_x, pieces),
         out_shape=[
             jax.ShapeDtypeStruct((part, width), BF16),
             jax.ShapeDtypeStruct((pairs, n_ty, 2, 2 * part), F32),
         ],
-        in_specs=[VMEM] * 18,
+        in_specs=[VMEM if n not in (2, 7, 8, 9, 14, 15) else pl.BlockSpec(memory_space=pl.ANY) for n in range(18)],
         out_specs=[VMEM] * 2,
         scratch_shapes=[
+            pltpu.VMEM(wq.shape, BF16),
+            pltpu.VMEM(w_pool_in.shape, BF16),
+            pltpu.VMEM(wqu.shape[::-1], BF16),
+            pltpu.VMEM(wkvu.shape, BF16),
+            pltpu.VMEM(w_out_attn.shape, BF16),
+            pltpu.VMEM(w_out_pool.shape, BF16),
+            dma((6,)),
             pltpu.VMEM((rows, wq.shape[1]), BF16),
             pltpu.VMEM((rows + 2 * HALO, pool_cols), BF16),
             pltpu.VMEM((n_dev, part + 16, rank), BF16),
@@ -428,7 +490,7 @@
             pltpu.VMEM((n_ty, part, width), BF16),
             pltpu.VMEM((n_ty, part, width), BF16),
             pltpu.VMEM((n_ty, part, width), BF16),
-            dma((n_chip,)), dma((n_dev,)), dma((n_chip,)),
+            dma((n_z,)), dma((n_z * n_ty,)), dma((n_chip * n_x,)), dma((n_dev,)), dma((n_chip,)),
             dma((n_tp,)), dma((n_tp,)), dma((n_tp,)), dma((n_tp,)), dma((2 * n_tp,)), dma((2,)),
             dma((n_ty * pieces,)), dma((n_ty * pieces,)), dma((n_ty * pieces,)), dma((n_ty * pieces,)),
         ],

time: 63.4 us -> 53.3 us (0.84)
  Pallas kernels: 59.4 us -> 49.3 us
    pallas_call x1, Pallas kernels: 59.4 us -> 49.3 us  [shards(): pl.pallas_call(functools.partial(layer_kernel, n_sp, n_tp, n_x, pieces),...]
where the time goes in v3:
time: 53.3 us; the launch traced here: 53.1 us
  Pallas kernels  49.3 us (92%)
  local copies, waits for them, and re-layouts  3.16 us (6%)
  between operations  0.65 us (1%)
    pallas_call x1, Pallas kernels, shards(): pl.pallas_call(functools.partial(layer_kernel, n_sp, n_tp, n_x, pieces),...  49.3 us
    unnamed x1, local copies, waits for them, and re-layouts  1.77 us

profile of v3, /device:TPU:0, one launch (start us, length us, event | category | flops | bytes accessed | tf_op | source)
XLA Modules:
  0.0 53.1 jit_solution(10099121384032980191)
XLA Ops:
  0.6 49.3 %shard_map.185 = (bf16[96,2048]{1,0:T(8,128)(2,1)}, f32[3,2,2,192]{3,2,1,0:T(2,128)}) custom-call(bf16[96,2048]{1,0:T(8,128)(2,1)} %x_ref.1, bf16[2048]{0:T(1024)(128)(2,1)} %gain_ref.1, bf16[2048,512]{1,0:T(8,128)(2,1)} %wq_hbm.1, bf16[512]{0:T(512)(128)(2,1)} %qlg_ref.1, bf16[2048,256]{1,0:T(8,128)(2,1)} %wkv_ref.1, bf16[256]{0:T(256)(128)(2,1)} %kvg_ref.1, ...), custom_call_target="tpu_custom_call" | custom-call | tf_op jit(solution)/shard_map/pallas_call | solution.py:464
  49.9 0.7 %copy.20 = f32[3,2,2,192]{3,2,1,0:T(2,128)S(1)} copy(f32[3,2,2,192]{3,1,2,0:T(2,128)} %bitcast.5) | data formatting | bytes 18432 | tf_op jit(solution)/shard_map/transpose | solution.py:501
  50.6 0.7 %reshape.7 = f32[6,384]{1,0:T(8,128)} reshape(f32[3,2,2,192]{3,2,1,0:T(2,128)S(1)} %copy.20) | data formatting | bytes 18432 | tf_op jit(solution)/shard_map/reshape | solution.py:501
  51.3 1.8 %copy.22 = bf16[96,2048]{1,0:T(8,128)(2,1)} copy(bf16[96,2048]{1,0:T(8,128)(2,1)} %get-tuple-element.8) | data formatting | bytes 786432
